TPU v7x, 32 devices: a whole 2x2x4 slice. The times are simulated.
32 devices in a mesh: grp: 2 (over y), kv: 4 (over z), tp: 4 (over x, core).
Axes of the slice: x: 2, y: 2, z: 4, core: 2. Of those that a mesh axis runs over, the one named last changes fastest.
Arguments:
- tokens: bfloat16 [512, 8, 4096], P('kv', 'grp'), parts along dimension 1, may hold values from -72 to 72
- lengths: int32 [8], P('grp'), parts along dimension 0, may hold values from 1 to 512, 768 in all
- chosen: int32 [8, 32, 8, 8], P('grp', 'tp', 'kv'), parts along dimension 0, may hold values from -1 to 7, as said below
- w_query: bfloat16 [4096, 2048], P(None, 'tp'), may hold values from -0.09375 to 0.09375
- w_key: bfloat16 [4096, 2048], P(None, 'tp'), may hold values from -0.09375 to 0.09375
- w_value: bfloat16 [4096, 2048], P(None, 'tp'), may hold values from -0.09375 to 0.09375
- w_gate: bfloat16 [4096, 2, 32], P(None, None, 'tp'), may hold values from -0.09375 to 0.09375
- pool_weights: float32 [2, 32, 64], replicated, may hold values from -1 to 1
- w_out: bfloat16 [2048, 4096], P(None, 'tp'), may hold values from -0.5 to 0.5
Outputs:
- mixed: bfloat16 [512, 8, 4096], P(('kv', 'tp'), 'grp'), parts along dimension 1
There are 2 independent parts, one for each index of `grp`. A program takes and returns all parts, laid end to end along the dimension named above; an argument that names none is the same for every part. Nothing has to cross between parts.
Inputs may be any that keep to these rules, and one draw needn't show every extreme that they name: `chosen`: for query block b the live slots hold min(8, b+1) distinct blocks, all <= b, among them b, b-1 (when b >= 1) and 0; the other slots are -1.
All inputs are finite; a program needn't handle non-finite values.
Results may differ from a plain program's by a relative error of at most 0.014.
Values may be sent and summed in bfloat16 or wider, within the bound.
No kernel may reach another device: no remote copies, remote signals or barrier semaphores. Data moves between devices by JAX's collectives and lax.ppermute only.
A program may use at most 128 MiB of HBM per device.

v0:
```python
from functools import partial
import jax
import jax.numpy as jnp
from jax import lax
from jax.sharding import PartitionSpec as P

HD = 64
QB = 64
L_CMP = 32
LOW_FILL = -1e30


def pooled_blocks(key_rows, pool_weight):
    row_count, seq_count, head_count, head_dim = key_rows.shape
    grouped = key_rows.reshape(row_count // L_CMP, L_CMP, seq_count, head_count, head_dim)
    return (grouped * pool_weight[None, :, None, None, :]).sum(1).astype(jnp.bfloat16)


def pooled_attend(queries, key_pooled, val_pooled, query_pos, lengths):
    head_dim = queries.shape[-1]
    cmp_end = jnp.arange(key_pooled.shape[0]) * L_CMP + L_CMP - 1
    scores = jnp.einsum(
        "qshd,cshd->shqc", queries, key_pooled, preferred_element_type=jnp.float32
    ) * head_dim ** (-0.5)
    usable = (cmp_end[None, None, :] <= query_pos[None, :, None]) & (
        cmp_end[None, None, :] < lengths[:, None, None]
    )
    usable = usable[:, None]
    row_top = jnp.max(jnp.where(usable, scores, LOW_FILL), axis=-1, keepdims=True)
    weights = jnp.where(usable, jnp.exp(scores - row_top), 0.0)
    totals = jnp.sum(weights, axis=-1)
    gathered = jnp.einsum(
        "shqc,cshd->shqd",
        weights.astype(jnp.bfloat16),
        val_pooled,
        preferred_element_type=jnp.float32,
    )
    return gathered / jnp.where(totals > 0, totals, 1.0)[..., None]


def fold_step(running, key_piece, begin_row, queries, chosen, query_pos, lengths):
    maxima, totals, weighted = running
    piece_keys, piece_values = key_piece
    head_dim = queries.shape[-1]
    key_pos = jnp.arange(piece_keys.shape[0])
    key_blk = key_pos // QB
    picked = jnp.any(chosen[..., None] == key_blk, axis=3)
    picked = jnp.repeat(picked, QB, axis=2)
    usable = (
        picked
        & (key_pos[None, None, None, :] <= query_pos[None, None, :, None])
        & (key_pos[None, None, None, :] < lengths[:, None, None, None])
    )
    scores = jnp.einsum(
        "qshd,kshd->shqk", queries, piece_keys, preferred_element_type=jnp.float32
    ) * head_dim ** (-0.5)
    new_max = jnp.maximum(maxima, jnp.max(jnp.where(usable, scores, LOW_FILL), axis=-1))
    weights = jnp.where(usable, jnp.exp(scores - new_max[..., None]), 0.0)
    shrink = jnp.exp(maxima - new_max)
    totals = jnp.sum(weights, axis=-1)
    weighted = jnp.einsum(
        "shqk,kshd->shqd",
        weights.astype(jnp.bfloat16),
        piece_values,
        preferred_element_type=jnp.float32,
    )
    return (new_max, totals, weighted)


def body(tokens, lengths, chosen, w_query, w_key, w_value, w_gate, pool_weights, w_out):
    row_count, seq_count, model_width = tokens.shape
    head_count = w_query.shape[1] // HD
    query_pos = lax.axis_index("kv") * row_count + jnp.arange(row_count)
    flat_rows = tokens.reshape(row_count * seq_count, model_width)

    def project(weight):
        product = jnp.dot(flat_rows, weight, preferred_element_type=jnp.float32)
        return product.astype(jnp.bfloat16).reshape(row_count, seq_count, head_count, HD)

    queries = project(w_query)
    key_rows = project(w_key)
    value_rows = project(w_value)
    gate_values = jax.nn.sigmoid(
        jnp.dot(
            flat_rows,
            w_gate.reshape(model_width, 2 * head_count),
            preferred_element_type=jnp.float32,
        )
    )
    gate_values = gate_values.reshape(row_count, seq_count, 2, head_count)
    key_pooled, val_pooled = (
        lax.all_gather(pooled_blocks(key_rows, pool_weights[0]), "kv", axis=0, tiled=True),
        lax.all_gather(pooled_blocks(value_rows, pool_weights[1]), "kv", axis=0, tiled=True),
    )
    start_state = (
        jnp.full((seq_count, head_count, row_count), LOW_FILL, jnp.float32),
        jnp.zeros((seq_count, head_count, row_count), jnp.float32),
        jnp.zeros((seq_count, head_count, row_count, HD), jnp.float32),
    )
    step_fn = partial(
        fold_step, queries=queries, chosen=chosen, query_pos=query_pos, lengths=lengths
    )
    maxima, totals, weighted = step_fn(
        start_state,
        (
            lax.all_gather(key_rows, "kv", axis=0, tiled=True),
            lax.all_gather(value_rows, "kv", axis=0, tiled=True),
        ),
        jnp.int32(0),
    )
    picked_out = weighted / jnp.where(totals > 0, totals, 1.0)[..., None]
    pooled_out = pooled_attend(queries, key_pooled, val_pooled, query_pos, lengths)
    combined = gate_values[:, :, 0, :, None] * pooled_out.transpose(2, 0, 1, 3) + gate_values[
        :, :, 1, :, None
    ] * picked_out.transpose(2, 0, 1, 3)
    live = query_pos[:, None] < lengths[None, :]
    attended = (
        jnp.where(live[:, :, None, None], combined, 0.0)
        .astype(jnp.bfloat16)
        .reshape(row_count, seq_count, head_count * HD)
    )
    group_count = lax.axis_size("tp")
    all_heads = lax.all_gather(attended, "tp", axis=2, tiled=True)
    group_width = head_count * HD
    col_width = w_out.shape[1]
    grouped_rows = all_heads.reshape(row_count * seq_count, group_count, group_width)
    grouped_weight = w_out.reshape(group_count, group_width, col_width)
    partial_cols = jnp.einsum(
        "rgk,gkc->rgc", grouped_rows, grouped_weight, preferred_element_type=jnp.float32
    )
    column_sum = jnp.sum(partial_cols.astype(jnp.bfloat16).astype(jnp.float32), axis=1)
    column_out = column_sum.astype(jnp.bfloat16).reshape(row_count, seq_count, col_width)
    return lax.all_to_all(column_out, "tp", split_axis=0, concat_axis=2, tiled=True)


def solution(mesh):
    placed = (
        P("kv", "grp", None),
        P("grp"),
        P("grp", "tp", "kv", None),
        P(None, "tp"),
        P(None, "tp"),
        P(None, "tp"),
        P(None, None, "tp"),
        P(),
        P(None, "tp"),
    )
    return jax.shard_map(
        body, mesh=mesh, in_specs=placed, out_specs=P(("kv", "tp"), "grp", None), check_vma=False
    )
```

profile of v0, /device:TPU:0, one launch (start us, length us, event | category | flops | bytes accessed | tf_op | source)
XLA Modules:
  0.0 181.1 jit_solution(17314178159223339070)
XLA Ops:
  6.5 7.0 %reshape.216 = bf16[512,4096]{1,0:T(8,128)(2,1)} reshape(bf16[128,4,4096]{2,1,0:T(4,128)(2,1)} %param.9) | data formatting | bytes 8388608 | tf_op jit(solution)/shard_map/reshape | solution.py:74
  13.5 5.8 %convolution_convert_fusion.1 = bf16[512,512]{1,0:T(8,128)(2,1)S(1)} fusion(bf16[512,4096]{1,0:T(8,128)(2,1)} %reshape.216, bf16[4096,512]{1,0:T(8,128)(2,1)} %param.13), kind=kOutput, calls=%fused_computation.19 | convolution fusion | flops 2147745792 | bytes 8912896 | tf_op jit(solution)/shard_map/dot_general | solution.py:77
  19.3 0.5 reshape.221
  19.8 1.9 %copy.57 = bf16[128,4,8,64]{0,3,2,1:T(8,128)(2,1)} copy(bf16[128,4,8,64]{3,2,1,0:T(8,128)(2,1)S(1)} %reshape.221) | data formatting | bytes 1048576 | tf_op jit(solution)/shard_map/reshape | solution.py:78
  21.7 0.0 all-gather.6.cloned.1.call-start
  21.8 5.8 %convolution_convert_fusion = bf16[512,512]{1,0:T(8,128)(2,1)S(1)} fusion(bf16[512,4096]{1,0:T(8,128)(2,1)} %reshape.216, bf16[4096,512]{1,0:T(8,128)(2,1)} %param.14), kind=kOutput, calls=%fused_computation.18 | convolution fusion | flops 2147745792 | bytes 8912896 | tf_op jit(solution)/shard_map/dot_general | solution.py:77
  27.6 0.5 reshape.222
  28.1 1.9 %copy.59 = bf16[128,4,8,64]{0,3,2,1:T(8,128)(2,1)} copy(bf16[128,4,8,64]{3,2,1,0:T(8,128)(2,1)S(1)} %reshape.222) | data formatting | bytes 1048576 | tf_op jit(solution)/shard_map/reshape | solution.py:78
  30.1 0.2 all-gather.8.cloned.1.call-start
  30.3 1.8 %reshape.228 = f32[4,32,4,8,64]{4,3,2,1,0:T(8,128)} reshape(bf16[512,512]{1,0:T(8,128)(2,1)S(1)} %convolution_convert_fusion) | data formatting | bytes 1572864 | tf_op jit(solution)/shard_map/convert_element_type | solution.py:16
  32.1 0.4 reshape.227
  32.6 3.5 %fusion.17 = f32[512,16]{0,1:T(8,128)S(1)} fusion(bf16[512,4096]{1,0:T(8,128)(2,1)} %reshape.216, bf16[4096,2,8]{0,2,1:T(8,128)(2,1)S(1)} %copy-done), kind=kOutput, calls=%fused_computation.30 | convolution fusion | flops 67133440 | bytes 4358144 | tf_op jit(solution)/shard_map/dot_general | solution.py:84
  36.1 0.1 copy.51
  36.2 0.3 reshape.218
  36.5 0.4 fusion.29
  37.0 0.1 copy.52
  37.0 0.1 copy.56
  37.2 5.8 %convolution_convert_fusion.2 = bf16[512,512]{1,0:T(8,128)(2,1)S(1)} fusion(bf16[512,4096]{1,0:T(8,128)(2,1)} %reshape.216, bf16[4096,512]{1,0:T(8,128)(2,1)} %param.12), kind=kOutput, calls=%fused_computation.20 | convolution fusion | flops 2147745792 | bytes 8912896 | tf_op jit(solution)/shard_map/dot_general | solution.py:77
  43.0 1.5 reshape.219
  44.5 2.2 %copy.53 = bf16[128,4,8,64]{0,3,2,1:T(8,128)(2,1)S(1)} copy(bf16[128,4,8,64]{3,2,1,0:T(8,128)(2,1)} %reshape.219) | data formatting | bytes 1048576 | tf_op jit(solution)/shard_map/reshape | solution.py:78
  46.8 1.9 %multiply_reduce_fusion = bf16[4,4,8,64]{3,2,1,0:T(8,128)(2,1)S(1)} fusion(f32[4,32,4,8,64]{4,3,2,1,0:T(8,128)} %reshape.228, f32[32,64]{1,0:T(8,128)S(1)} %get-tuple-element.9), kind=kLoop, calls=%fused_computation.9 | loop fusion | flops 516096 | bytes 1073152 | tf_op jit(solution)/shard_map/reduce_sum | solution.py:16
  48.6 16.0 %all_gather.16 = bf16[16,4,8,64]{3,2,1,0:T(8,128)(2,1)S(1)} all-gather(bf16[4,4,8,64]{3,2,1,0:T(8,128)(2,1)S(1)} %multiply_reduce_fusion), channel_id=1, replica_groups=mesh['grp'=2,'kv'=4,'tp'=4] {'kv'}, dimensions={0}, use_global_device_ids=true | all-gather | bytes 81920 | tf_op jit(solution)/shard_map/all_gather | solution.py:93
  64.6 0.3 multiply_reduce_fusion.1
  64.9 18.8 %all_gather.15 = bf16[16,4,8,64]{3,2,1,0:T(8,128)(2,1)S(1)} all-gather(bf16[4,4,8,64]{3,2,1,0:T(8,128)(2,1)S(1)} %multiply_reduce_fusion.1), channel_id=1, replica_groups=mesh['grp'=2,'kv'=4,'tp'=4] {'kv'}, dimensions={0}, use_global_device_ids=true | all-gather | bytes 81920 | tf_op jit(solution)/shard_map/all_gather | solution.py:92
  83.7 0.5 compare_reduce_fusion
  84.2 0.1 broadcast_compare_fusion.1
  84.3 0.1 broadcast_compare_fusion.2
  84.3 0.1 iota_compare_fusion.1
  84.4 0.1 broadcast_compare_fusion
  84.5 0.1 broadcast_and_fusion
  84.6 0.3 convolution_multiply_fusion
  84.8 0.1 fusion.30
  85.0 0.1 iota_compare_fusion
  85.1 0.0 all-gather.4.cloned.1.call-done
  85.1 4.3 %select_reduce_fusion = (f32[4,8,128]{2,1,0:T(8,128)S(1)}, f32[4,8,128,512]{3,2,1,0:T(8,128)S(1)}) fusion(pred[4,512]{1,0:T(4,128)(4,1)S(1)} %iota_compare_fusion.1, pred[128,512]{1,0:T(8,128)(4,1)S(1)} %iota_compare_fusion, pred[4,8,2,512]{3,2,1,0:T(4,128)(4,1)S(1)} %compare_reduce_fusion, bf16[128,4,8,64]{0,3,2,1:T(8,128)(2,1)S(1)} %copy.53, ...), kind=kOutput, calls=%fused_computation.2 | convolution fusion | flops 278917120 | bytes 11126784 | tf_op jit(solution)/shard_map/qshd,kshd->shqk/dot_general | solution.py:54
  89.4 4.5 %fusion.2 = (f32[4,8,128]{2,1,0:T(8,128)S(1)}, bf16[4,8,128,512]{3,2,1,0:T(8,128)(2,1)}) fusion(f32[4,8,128,512]{3,2,1,0:T(8,128)S(1)} %get-tuple-element.12, f32[4,8,128]{2,1,0:T(8,128)S(1)} %broadcast_maximum_fusion, pred[4,512]{1,0:T(4,128)(4,1)S(1)} %iota_compare_fusion.1, pred[128,512]{1,0:T(8,128)(4,1)S(1)} %iota_compare_fusion, ...), kind=kLoop, calls=%fused_computation.5 | loop fusion | flops 14675968 | bytes 12716032 | tf_op jit(solution)/shard_map/reduce_sum | solution.py:60
  93.9 25.4 %all-gather.6.cloned.1.call-done = bf16[512,4,8,64]{0,3,2,1:T(8,128)(2,1)} async-done(((bf16[128,4,8,64]{0,3,2,1:T(8,128)(2,1)}), bf16[512,4,8,64]{0,3,2,1:T(8,128)(2,1)}) %all-gather.6.cloned.1.call-update) | async-done | bytes 2097168 | tf_op jit(solution)/shard_map/all_gather | solution.py:107
  119.3 4.4 %fusion.11 = f32[128,4,8,64]{0,3,2,1:T(8,128)S(1)} fusion(bf16[4,8,128,512]{3,2,1,0:T(8,128)(2,1)} %get-tuple-element.6, bf16[512,4,8,64]{0,3,2,1:T(8,128)(2,1)} %all-gather.6.cloned.1.call-done, f32[128,4,8]{0,2,1:T(8,128)S(1)} %compare_select_fusion, f32[128,4,8]{0,2,1:T(8,128)S(1)} %copy.56), kind=kOutput, calls=%fused_computation.22 | convolution fusion | flops 268959744 | bytes 7372800 | tf_op jit(solution)/shard_map/shqk,kshd->shqd/dot_general | solution.py:61
  123.7 0.4 fusion.9
  124.1 1.2 copy.60
  125.3 21.4 %all-gather.8.cloned.1.call-done = bf16[128,4,2048]{2,1,0:T(4,128)(2,1)} async-done(((bf16[128,4,512]{2,1,0:T(4,128)(2,1)}), bf16[128,4,2048]{2,1,0:T(4,128)(2,1)}) %all-gather.8.cloned.1.call-update) | async-done | bytes 2097168 | tf_op jit(solution)/shard_map/all_gather | solution.py:123
  146.7 3.1 %reshape.224 = bf16[512,4,512]{2,1,0:T(4,128)(2,1)S(1)} reshape(bf16[128,4,2048]{2,1,0:T(4,128)(2,1)} %all-gather.8.cloned.1.call-done) | data formatting | bytes 4194304 | tf_op jit(solution)/shard_map/reshape | solution.py:126
  149.9 4.6 %convert_reduce_fusion = bf16[512,1024]{1,0:T(8,128)(2,1)S(1)} fusion(bf16[4,512,1024]{2,1,0:T(8,128)(2,1)} %bitcast.66, bf16[512,4,512]{2,1,0:T(4,128)(2,1)S(1)} %reshape.224), kind=kOutput, calls=%fused_computation.7 | convolution fusion | flops 2151153664 | bytes 7340032 | tf_op jit(solution)/shard_map/rgk,gkc->rgc/dot_general | solution.py:128
  154.5 0.4 reshape.226
  154.9 16.9 %all_to_all.18 = bf16[128,4,1024]{2,1,0:T(4,128)(2,1)S(1)} all-to-all(bf16[128,4,1024]{2,1,0:T(4,128)(2,1)S(1)} %reshape.226), channel_id=1, replica_groups=mesh['grp'=2,'kv'=4,'tp'=4] {'tp'}, dimensions={0} | all-to-all | bytes 2097152 | tf_op jit(solution)/shard_map/all_to_all | solution.py:133
  171.8 0.3 copy.62
  172.1 0.8 copy.65
  172.9 1.6 reshape.229
  (21 shorter events, 0.1 us)
Async XLA Ops:
  6.5 26.1 %copy-start = (bf16[4096,2,8]{0,2,1:T(8,128)(2,1)S(1)}, bf16[4096,2,8]{0,2,1:T(8,128)(2,1)}, u32[]{:S(2)}) copy-start(bf16[4096,2,8]{0,2,1:T(8,128)(2,1)} %param.15) | copy-start | bytes 393220
  6.5 78.6 %all-gather.4.cloned.1.call-start = ((), (), s32[]{:S(2)}) async-start(), calls=%async_computation.1 | async-start | bytes 2621440 | tf_op jit(solution)/shard_map/all_gather | solution.py:106
  21.7 97.5 %all-gather.6.cloned.1.call-start = ((), (), s32[]{:S(2)}) async-start(), calls=%async_computation.2 | async-start | bytes 2621440 | tf_op jit(solution)/shard_map/all_gather | solution.py:107
  27.6 5.0 %copy-start.3 = (f32[2,32,64]{2,1,0:T(8,128)S(1)}, f32[2,32,64]{2,1,0:T(8,128)}, u32[]{:S(2)}) copy-start(f32[2,32,64]{2,1,0:T(8,128)} %param.16) | copy-start | bytes 49156
  30.1 116.6 %all-gather.8.cloned.1.call-start = ((), (), s32[]{:S(2)}) async-start(), calls=%async_computation.3 | async-start | bytes 2621440 | tf_op jit(solution)/shard_map/all_gather | solution.py:123
  43.0 40.7 %copy-start.2 = (s32[4,8,2,8]{3,2,1,0:T(2,128)S(1)}, s32[4,8,2,8]{3,2,1,0:T(2,128)}, u32[]{:S(2)}) copy-start(s32[4,8,2,8]{3,2,1,0:T(2,128)} %param.11) | copy-start | bytes 6148
  43.0 41.2 %copy-start.4 = (s32[4]{0:T(128)S(1)}, s32[4]{0:T(128)}, u32[]{:S(2)}) copy-start(s32[4]{0:T(128)} %param.10) | copy-start | bytes 52
  154.5 20.1 %copy-start.1 = (bf16[4096,2,8]{0,2,1:T(8,128)(2,1)S(1)}, bf16[4096,2,8]{0,2,1:T(8,128)(2,1)}, u32[]{:S(2)}) copy-start(bf16[4096,2,8]{0,2,1:T(8,128)(2,1)} %param.15) | copy-start | bytes 393220
Sparse Core Ops, SparseCore 0:
  21.9 51.1 all-gather.3
  74.6 44.6 all-gather.5
  125.4 21.2 all-gather.7
where the time goes:
time: 182 us; the launch traced here: 181 us
  blocking collectives  51.6 us (28%)
  waiting for transfers between devices  46.9 us (26%)
  matrix products  34.8 us (19%)
  local copies, waits for them, and re-layouts  26.4 us (15%)
  between operations  13.4 us (7%)
  other arithmetic  7.72 us (4%)
    all_gather x1, waiting for transfers between devices, body(): lax.all_gather(value_rows, 'kv', axis=0, tiled=True)  25.4 us
    all_gather x1, waiting for transfers between devices, body(): all_heads = lax.all_gather(attended, 'tp', axis=2, tiled=True)  21.4 us
    all_gather x1, blocking collectives, body(): lax.all_gather(pooled_blocks(key_rows, pool_weights[0]), 'kv', axis=0, ti...  18.8 us
    dot_general x3, matrix products, project(): product = jnp.dot(flat_rows, weight, preferred_element_type=jnp.float32)  17.4 us
    all_to_all x1, blocking collectives, body(): lax.all_to_all(column_out, 'tp', split_axis=0, concat_axis=2, tiled=True)  16.9 us
    all_gather x1, blocking collectives, body(): lax.all_gather(pooled_blocks(value_rows, pool_weights[1]), 'kv', axis=0,...  16 us
    reshape x6, local copies, waits for them, and re-layouts, project(): product.astype(jnp.bfloat16).reshape(row_count, seq_count, head_count, HD)  8.64 us
    reshape x1, local copies, waits for them, and re-layouts, body(): flat_rows = tokens.reshape(row_count * seq_count, model_width)  6.95 us
  transfers between devices with their start and end apart: 3, of which 2 were waited for; matrix products, arithmetic and copies ran while one was open for 20% of the time, Pallas kernels for 0%

commit v1 on v0

--- a/solution.py
+++ b/solution.py
@@ -120,7 +120,12 @@
         .reshape(row_count, seq_count, head_count * HD)
     )
     group_count = lax.axis_size("tp")
-    all_heads = lax.all_gather(attended, "tp", axis=2, tiled=True)
+    ring = [attended]
+    for hop in range(3):
+        ring.append(lax.ppermute(ring[-1], "tp", [(dev, (dev + 1) % 4) for dev in range(4)]))
+    all_heads = jnp.roll(
+        jnp.concatenate(ring[::-1], axis=2), (lax.axis_index("tp") + 1) * ring[0].shape[2], axis=2
+    )
     group_width = head_count * HD
     col_width = w_out.shape[1]
     grouped_rows = all_heads.reshape(row_count * seq_count, group_count, group_width)

time: 182 us -> 189 us (1.038)
  waiting for transfers between devices: 46.9 us -> 51.1 us
    ppermute x0 -> x3, waiting for transfers between devices: none -> 25.8 us  [body(): lax.ppermute(ring[-1], 'tp', [(dev, (dev + 1) % 4) for dev in range(4)])]
    all_gather x1 -> x0, waiting for transfers between devices: 21.4 us -> none  [body(): all_heads = lax.all_gather(attended, 'tp', axis=2, tiled=True)]
  transfers between devices with their start and end apart: 3 -> 5, of which waited for: 2 -> 4; matrix products, arithmetic and copies ran while one was open for 20% -> 20% of each run, Pallas kernels for 0% -> 0%
where the time goes in v1:
time: 189 us; the launch traced here: 188 us
  blocking collectives  52 us (28%)
  waiting for transfers between devices  51.1 us (27%)
  matrix products  35.5 us (19%)
  local copies, waits for them, and re-layouts  28 us (15%)
  between operations  13.7 us (7%)
  other arithmetic  7.72 us (4%)
    ppermute x3, waiting for transfers between devices, body(): lax.ppermute(ring[-1], 'tp', [(dev, (dev + 1) % 4) for dev in range(4)])  25.8 us
    all_gather x1, waiting for transfers between devices, body(): lax.all_gather(value_rows, 'kv', axis=0, tiled=True)  25.3 us
    all_gather x1, blocking collectives, body(): lax.all_gather(pooled_blocks(key_rows, pool_weights[0]), 'kv', axis=0, ti...  19 us
    dot_general x3, matrix products, project(): product = jnp.dot(flat_rows, weight, preferred_element_type=jnp.float32)  17.4 us
    all_to_all x1, blocking collectives, body(): lax.all_to_all(column_out, 'tp', split_axis=0, concat_axis=2, tiled=True)  17 us
    all_gather x1, blocking collectives, body(): lax.all_gather(pooled_blocks(value_rows, pool_weights[1]), 'kv', axis=0,...  16 us
    reshape x6, local copies, waits for them, and re-layouts, project(): product.astype(jnp.bfloat16).reshape(row_count, seq_count, head_count, HD)  8.64 us
    reshape x1, local copies, waits for them, and re-layouts, body(): flat_rows = tokens.reshape(row_count * seq_count, model_width)  6.95 us
  transfers between devices with their start and end apart: 5, of which 4 were waited for; matrix products, arithmetic and copies ran while one was open for 20% of the time, Pallas kernels for 0%

profile of v1, /device:TPU:0, one launch (start us, length us, event | category | flops | bytes accessed | tf_op | source)
XLA Modules:
  0.0 188.3 jit_solution(14486756463867456871)
XLA Ops:
  6.5 7.0 %reshape.216 = bf16[512,4096]{1,0:T(8,128)(2,1)} reshape(bf16[128,4,4096]{2,1,0:T(4,128)(2,1)} %param.9) | data formatting | bytes 8388608 | tf_op jit(solution)/shard_map/reshape | solution.py:74
  13.5 5.8 %convolution_convert_fusion.1 = bf16[512,512]{1,0:T(8,128)(2,1)S(1)} fusion(bf16[512,4096]{1,0:T(8,128)(2,1)} %reshape.216, bf16[4096,512]{1,0:T(8,128)(2,1)} %param.13), kind=kOutput, calls=%fused_computation.19 | convolution fusion | flops 2147745792 | bytes 8912896 | tf_op jit(solution)/shard_map/dot_general | solution.py:77
  19.3 0.5 reshape.221
  19.8 1.9 %copy.63 = bf16[128,4,8,64]{0,3,2,1:T(8,128)(2,1)} copy(bf16[128,4,8,64]{3,2,1,0:T(8,128)(2,1)S(1)} %reshape.221) | data formatting | bytes 1048576 | tf_op jit(solution)/shard_map/reshape | solution.py:78
  21.7 0.2 all-gather.5.cloned.1.call-start
  22.0 5.8 %convolution_convert_fusion = bf16[512,512]{1,0:T(8,128)(2,1)S(1)} fusion(bf16[512,4096]{1,0:T(8,128)(2,1)} %reshape.216, bf16[4096,512]{1,0:T(8,128)(2,1)} %param.14), kind=kOutput, calls=%fused_computation.18 | convolution fusion | flops 2147745792 | bytes 8912896 | tf_op jit(solution)/shard_map/dot_general | solution.py:77
  27.8 0.5 reshape.222
  28.3 1.9 %copy.65 = bf16[128,4,8,64]{0,3,2,1:T(8,128)(2,1)} copy(bf16[128,4,8,64]{3,2,1,0:T(8,128)(2,1)S(1)} %reshape.222) | data formatting | bytes 1048576 | tf_op jit(solution)/shard_map/reshape | solution.py:78
  30.3 1.8 reshape.228
  32.1 0.4 reshape.227
  32.5 3.5 %fusion.17 = f32[512,16]{0,1:T(8,128)S(1)} fusion(bf16[512,4096]{1,0:T(8,128)(2,1)} %reshape.216, bf16[4096,2,8]{0,2,1:T(8,128)(2,1)S(1)} %copy-done), kind=kOutput, calls=%fused_computation.30 | convolution fusion | flops 67133440 | bytes 4358144 | tf_op jit(solution)/shard_map/dot_general | solution.py:84
  36.2 0.3 reshape.218
  36.5 0.4 fusion.29
  37.1 5.8 %convolution_convert_fusion.2 = bf16[512,512]{1,0:T(8,128)(2,1)S(1)} fusion(bf16[512,4096]{1,0:T(8,128)(2,1)} %reshape.216, bf16[4096,512]{1,0:T(8,128)(2,1)} %param.12), kind=kOutput, calls=%fused_computation.20 | convolution fusion | flops 2147745792 | bytes 8912896 | tf_op jit(solution)/shard_map/dot_general | solution.py:77
  43.0 1.5 reshape.219
  44.5 2.2 %copy.59 = bf16[128,4,8,64]{0,3,2,1:T(8,128)(2,1)S(1)} copy(bf16[128,4,8,64]{3,2,1,0:T(8,128)(2,1)} %reshape.219) | data formatting | bytes 1048576 | tf_op jit(solution)/shard_map/reshape | solution.py:78
  46.7 1.9 multiply_reduce_fusion
  48.6 16.0 %all_gather.13 = bf16[16,4,8,64]{3,2,1,0:T(8,128)(2,1)S(1)} all-gather(bf16[4,4,8,64]{3,2,1,0:T(8,128)(2,1)S(1)} %multiply_reduce_fusion), channel_id=1, replica_groups=mesh['grp'=2,'kv'=4,'tp'=4] {'kv'}, dimensions={0}, use_global_device_ids=true | all-gather | bytes 81920 | tf_op jit(solution)/shard_map/all_gather | solution.py:93
  64.6 0.3 multiply_reduce_fusion.1
  64.8 19.0 %all_gather.12 = bf16[16,4,8,64]{3,2,1,0:T(8,128)(2,1)S(1)} all-gather(bf16[4,4,8,64]{3,2,1,0:T(8,128)(2,1)S(1)} %multiply_reduce_fusion.1), channel_id=1, replica_groups=mesh['grp'=2,'kv'=4,'tp'=4] {'kv'}, dimensions={0}, use_global_device_ids=true | all-gather | bytes 81920 | tf_op jit(solution)/shard_map/all_gather | solution.py:92
  83.8 0.5 compare_reduce_fusion
  84.7 0.3 convolution_multiply_fusion
  85.0 0.1 fusion.30
  85.3 4.3 %select_reduce_fusion = (f32[4,8,128]{2,1,0:T(8,128)S(1)}, f32[4,8,128,512]{3,2,1,0:T(8,128)S(1)}) fusion(pred[4,512]{1,0:T(4,128)(4,1)S(1)} %iota_compare_fusion.1, pred[128,512]{1,0:T(8,128)(4,1)S(1)} %iota_compare_fusion, pred[4,8,2,512]{3,2,1,0:T(4,128)(4,1)S(1)} %compare_reduce_fusion, bf16[128,4,8,64]{0,3,2,1:T(8,128)(2,1)S(1)} %copy.59, ...), kind=kOutput, calls=%fused_computation.2 | convolution fusion | flops 278917120 | bytes 11126784 | tf_op jit(solution)/shard_map/qshd,kshd->shqk/dot_general | solution.py:54
  89.5 4.5 %fusion.2 = (f32[4,8,128]{2,1,0:T(8,128)S(1)}, bf16[4,8,128,512]{3,2,1,0:T(8,128)(2,1)}) fusion(f32[4,8,128,512]{3,2,1,0:T(8,128)S(1)} %get-tuple-element.12, f32[4,8,128]{2,1,0:T(8,128)S(1)} %broadcast_maximum_fusion, pred[4,512]{1,0:T(4,128)(4,1)S(1)} %iota_compare_fusion.1, pred[128,512]{1,0:T(8,128)(4,1)S(1)} %iota_compare_fusion, ...), kind=kLoop, calls=%fused_computation.5 | loop fusion | flops 14675968 | bytes 12716032 | tf_op jit(solution)/shard_map/reduce_sum | solution.py:60
  94.0 25.3 %all-gather.5.cloned.1.call-done = bf16[512,4,8,64]{0,3,2,1:T(8,128)(2,1)} async-done(((bf16[128,4,8,64]{0,3,2,1:T(8,128)(2,1)}), bf16[512,4,8,64]{0,3,2,1:T(8,128)(2,1)}) %all-gather.5.cloned.1.call-update) | async-done | bytes 2097168 | tf_op jit(solution)/shard_map/all_gather | solution.py:107
  119.3 4.4 %fusion.11 = f32[128,4,8,64]{0,3,2,1:T(8,128)S(1)} fusion(bf16[4,8,128,512]{3,2,1,0:T(8,128)(2,1)} %get-tuple-element.6, bf16[512,4,8,64]{0,3,2,1:T(8,128)(2,1)} %all-gather.5.cloned.1.call-done, f32[128,4,8]{0,2,1:T(8,128)S(1)} %compare_select_fusion, f32[128,4,8]{0,2,1:T(8,128)S(1)} %copy.62), kind=kOutput, calls=%fused_computation.22 | convolution fusion | flops 268959744 | bytes 7372800 | tf_op jit(solution)/shard_map/shqk,kshd->shqd/dot_general | solution.py:61
  123.7 0.4 fusion.9
  124.1 0.4 copy.66
  124.6 8.6 %collective-permute-done = bf16[128,4,512]{2,1,0:T(4,128)(2,1)S(1)} collective-permute-done((bf16[128,4,512]{2,1,0:T(4,128)(2,1)S(1)}, bf16[128,4,512]{2,1,0:T(4,128)(2,1)S(1)}, u32[]{:S(2)}, u32[]{:S(2)}) %collective-permute-start) | collective-permute-done | bytes 524320 | tf_op jit(solution)/shard_map/ppermute | solution.py:125
  133.2 8.6 %collective-permute-done.1 = bf16[128,4,512]{2,1,0:T(4,128)(2,1)S(1)} collective-permute-done((bf16[128,4,512]{2,1,0:T(4,128)(2,1)S(1)}, bf16[128,4,512]{2,1,0:T(4,128)(2,1)S(1)}, u32[]{:S(2)}, u32[]{:S(2)}) %collective-permute-start.1) | collective-permute-done | bytes 524320 | tf_op jit(solution)/shard_map/ppermute | solution.py:125
  141.8 8.6 %collective-permute-done.2 = bf16[128,4,512]{2,1,0:T(4,128)(2,1)S(1)} collective-permute-done((bf16[128,4,512]{2,1,0:T(4,128)(2,1)S(1)}, bf16[128,4,512]{2,1,0:T(4,128)(2,1)S(1)}, u32[]{:S(2)}, u32[]{:S(2)}) %collective-permute-start.2) | collective-permute-done | bytes 524320 | tf_op jit(solution)/shard_map/ppermute | solution.py:125
  150.4 0.3 constant_dynamic-update-slice_fusion.7
  150.7 0.2 constant_dynamic-update-slice_fusion.6
  150.9 0.2 constant_dynamic-update-slice_fusion.5
  151.2 0.2 constant_dynamic-update-slice_fusion.4
  151.4 0.2 constant_dynamic-update-slice_fusion.3
  151.6 0.2 constant_dynamic-update-slice_fusion.2
  151.9 0.2 constant_dynamic-update-slice_fusion.1
  152.1 0.2 constant_dynamic-update-slice_fusion
  152.4 1.0 constant_dynamic-slice_fusion
  153.4 2.7 %reshape.224 = bf16[512,4,512]{2,1,0:T(4,128)(2,1)} reshape(bf16[128,4,2048]{2,1,0:T(4,128)(2,1)S(1)} %constant_dynamic-slice_fusion) | data formatting | bytes 4194304 | tf_op jit(solution)/shard_map/reshape | solution.py:131
  156.0 5.3 %convert_reduce_fusion = bf16[512,1024]{1,0:T(8,128)(2,1)S(1)} fusion(bf16[4,512,1024]{2,1,0:T(8,128)(2,1)} %bitcast.66, bf16[512,4,512]{2,1,0:T(4,128)(2,1)} %reshape.224), kind=kOutput, calls=%fused_computation.7 | convolution fusion | flops 2151153664 | bytes 7340032 | tf_op jit(solution)/shard_map/rgk,gkc->rgc/dot_general | solution.py:133
  161.3 0.4 reshape.226
  161.7 17.0 %all_to_all.18 = bf16[128,4,1024]{2,1,0:T(4,128)(2,1)S(1)} all-to-all(bf16[128,4,1024]{2,1,0:T(4,128)(2,1)S(1)} %reshape.226), channel_id=1, replica_groups=mesh['grp'=2,'kv'=4,'tp'=4] {'tp'}, dimensions={0} | all-to-all | bytes 2097152 | tf_op jit(solution)/shard_map/all_to_all | solution.py:138
  178.7 0.3 copy.70
  179.1 0.8 copy.73
  179.9 1.6 reshape.229
  (33 shorter events, 1.0 us)
Async XLA Ops:
  6.5 26.0 %copy-start = (bf16[4096,2,8]{0,2,1:T(8,128)(2,1)S(1)}, bf16[4096,2,8]{0,2,1:T(8,128)(2,1)}, u32[]{:S(2)}) copy-start(bf16[4096,2,8]{0,2,1:T(8,128)(2,1)} %param.15) | copy-start | bytes 393220
  6.5 78.7 %all-gather.3.cloned.1.call-start = ((), (), s32[]{:S(2)}) async-start(), calls=%async_computation.1 | async-start | bytes 2621440 | tf_op jit(solution)/shard_map/all_gather | solution.py:106
  21.7 97.5 %all-gather.5.cloned.1.call-start = ((), (), s32[]{:S(2)}) async-start(), calls=%async_computation.2 | async-start | bytes 2621440 | tf_op jit(solution)/shard_map/all_gather | solution.py:107
  27.8 4.7 %copy-start.3 = (f32[2,32,64]{2,1,0:T(8,128)S(1)}, f32[2,32,64]{2,1,0:T(8,128)}, u32[]{:S(2)}) copy-start(f32[2,32,64]{2,1,0:T(8,128)} %param.16) | copy-start | bytes 49156
  42.9 40.9 %copy-start.2 = (s32[4,8,2,8]{3,2,1,0:T(2,128)S(1)}, s32[4,8,2,8]{3,2,1,0:T(2,128)}, u32[]{:S(2)}) copy-start(s32[4,8,2,8]{3,2,1,0:T(2,128)} %param.11) | copy-start | bytes 6148
  42.9 41.4 %copy-start.4 = (s32[4]{0:T(128)S(1)}, s32[4]{0:T(128)}, u32[]{:S(2)}) copy-start(s32[4]{0:T(128)} %param.10) | copy-start | bytes 52
  124.5 8.7 %collective-permute-start = (bf16[128,4,512]{2,1,0:T(4,128)(2,1)S(1)}, bf16[128,4,512]{2,1,0:T(4,128)(2,1)S(1)}, u32[]{:S(2)}, u32[]{:S(2)}) collective-permute-start(bf16[128,4,512]{2,1,0:T(4,128)(2,1)S(1)} %copy.66), channel_id=1, source_target_pairs={{0,1},{1,2},{2,3},{3,0},{4,5},{5,6},{6,7},{7,4},{8,9},{9,10},{10,1... | collective-permute-start | bytes 1572872 | tf_op jit(solution)/shard_map/ppermute | solution.py:125
  133.2 8.6 %collective-permute-start.1 = (bf16[128,4,512]{2,1,0:T(4,128)(2,1)S(1)}, bf16[128,4,512]{2,1,0:T(4,128)(2,1)S(1)}, u32[]{:S(2)}, u32[]{:S(2)}) collective-permute-start(bf16[128,4,512]{2,1,0:T(4,128)(2,1)S(1)} %collective-permute-done), channel_id=1, source_target_pairs={{0,1},{1,2},{2,3},{3,0},{4,5},{5,6},{6,7},{7,4},{8,9},{9,10},{10,1... | collective-permute-start | bytes 1572872 | tf_op jit(solution)/shard_map/ppermute | solution.py:125
  141.8 8.6 %collective-permute-start.2 = (bf16[128,4,512]{2,1,0:T(4,128)(2,1)S(1)}, bf16[128,4,512]{2,1,0:T(4,128)(2,1)S(1)}, u32[]{:S(2)}, u32[]{:S(2)}) collective-permute-start(bf16[128,4,512]{2,1,0:T(4,128)(2,1)S(1)} %collective-permute-done.1), channel_id=1, source_target_pairs={{0,1},{1,2},{2,3},{3,0},{4,5},{5,6},{6,7},{7,4},{8,9},{9,10},{10,1... | collective-permute-start | bytes 1572872 | tf_op jit(solution)/shard_map/ppermute | solution.py:125
  161.3 20.2 %copy-start.1 = (bf16[4096,2,8]{0,2,1:T(8,128)(2,1)S(1)}, bf16[4096,2,8]{0,2,1:T(8,128)(2,1)}, u32[]{:S(2)}) copy-start(bf16[4096,2,8]{0,2,1:T(8,128)(2,1)} %param.15) | copy-start | bytes 393220
Sparse Core Ops, SparseCore 0:
  21.9 51.5 all-gather.2
  75.0 44.2 all-gather.4
